TPU v7x, 256 devices: a whole 4x4x8 slice. The times are simulated.
256 devices in a mesh: sp: 16 (over y, x), tp: 16 (over z, core).
Axes of the slice: x: 4, y: 4, z: 8, core: 2. Of those that a mesh axis runs over, the one named last changes fastest.
Arguments:
- conv_value: bfloat16 [49152, 2048], P('sp', 'tp'), may hold values from -48 to 48
- conv_gate: bfloat16 [49152, 2048], P('sp', 'tp'), may hold values from -6 to 6
- doc_ids: int32 [49152], P('sp'), may hold values from 0 to 15, never falling along the last dimension, each value on 1 to 9216 neighbouring positions
- conv_kernel: bfloat16 [31, 2048], P(None, 'tp'), may hold values from -1 to 1
- norm_gain_conv: float32 [2048], replicated, may hold values from 0.1 to 1.9
- norm_bias_conv: float32 [2048], replicated, may hold values from -3 to 3
- proj_weight: bfloat16 [2048, 2048], P('tp'), may hold values from -0.125 to 0.125
- residual: bfloat16 [49152, 2048], P(('sp', 'tp')), may hold values from -6 to 6
- norm_gain_moe: float32 [2048], replicated, may hold values from 0.1 to 1.9
- group_router: bfloat16 [2048, 2], replicated, may hold values from -0.125 to 0.125
- expert_router: bfloat16 [2048, 16], replicated, may hold values from -0.125 to 0.125
- routing: int32 [49152, 2], P(('sp', 'tp')), may hold values from 0 to 15, as said below
- expert_gate_w: bfloat16 [16, 2048, 512], P('sp'), may hold values from -0.125 to 0.125
- expert_up_w: bfloat16 [16, 2048, 512], P('sp'), may hold values from -0.125 to 0.125
- expert_down_w: bfloat16 [16, 512, 2048], P('sp'), may hold values from -0.25 to 0.25
Outputs:
- output: bfloat16 [49152, 2048], P(('sp', 'tp'))
Inputs may be any that keep to these rules, and one draw needn't show every extreme that they name: `routing`: both numbers of a row are different experts of one group (expert // 8); within the rows of one device (aligned blocks of 192 rows) every expert is named exactly 24 times.
All inputs are finite; a program needn't handle non-finite values.
Results may differ from a plain program's by a relative error of at most 0.015.
Values may be sent and summed in bfloat16 or wider, within the bound.
No kernel may reach another device: no remote copies, remote signals or barrier semaphores. Data moves between devices by JAX's collectives and lax.ppermute only.
A program may use at most 64 MiB of HBM per device.

v0:
```python
import jax
import jax.numpy as jnp
from jax import lax
from jax.sharding import PartitionSpec as P

epsilon = 1e-06


def shifted(array, axis, by):
    count = lax.axis_size(axis)
    pairs = [(i, i + by) for i in range(count) if 0 <= i + by < count]
    return lax.ppermute(array, axis, pairs)


def project_rows(activated_rows, proj_weight):
    return jnp.dot(
        activated_rows,
        lax.all_gather(proj_weight, "tp", axis=0, tiled=True),
        preferred_element_type=jnp.float32,
    )


def body(
    conv_value,
    conv_gate,
    doc_ids,
    conv_kernel,
    norm_gain_conv,
    norm_bias_conv,
    proj_weight,
    residual,
    norm_gain_moe,
    group_router,
    expert_router,
    routing,
    expert_gate_w,
    expert_up_w,
    expert_down_w,
):
    local_tokens, local_width = conv_value.shape
    kernel_taps = conv_kernel.shape[0]
    rim_width = kernel_taps - 1
    gated_values = (
        conv_value.astype(jnp.float32) * jax.nn.sigmoid(conv_gate.astype(jnp.float32))
    ).astype(jnp.bfloat16)
    rim_values, rim_ids = shifted(
        (gated_values[local_tokens - rim_width :], doc_ids[local_tokens - rim_width :]), "sp", 1
    )
    padded = jnp.concatenate([rim_values, gated_values], axis=0)
    padded_ids = jnp.concatenate([rim_ids, doc_ids], axis=0)
    kernel = conv_kernel.astype(jnp.float32)
    summed = jnp.zeros((local_tokens, local_width), jnp.float32)
    for tap in range(kernel_taps):
        same_doc = padded_ids[tap : tap + local_tokens] == doc_ids
        summed = summed + jnp.where(
            same_doc[:, None],
            padded[tap : tap + local_tokens].astype(jnp.float32) * kernel[tap][None, :],
            jnp.float32(0.0),
        )
    convolved = summed.astype(jnp.bfloat16)
    raw_rows = lax.all_to_all(convolved, "tp", split_axis=0, concat_axis=1, tiled=True)
    raw_values = raw_rows.astype(jnp.float32)
    average = jnp.mean(raw_values, axis=1, keepdims=True)
    centered = raw_values - average
    variance = jnp.mean(centered * centered, axis=1, keepdims=True)
    moved_rows = jax.nn.silu(
        centered * lax.rsqrt(variance + epsilon) * norm_gain_conv + norm_bias_conv
    ).astype(jnp.bfloat16)
    projected = project_rows(moved_rows, proj_weight)
    state_values = residual.astype(jnp.float32) + projected
    hidden_state = state_values.astype(jnp.bfloat16)
    state_values = hidden_state.astype(jnp.float32)
    normed = (
        state_values
        * lax.rsqrt(jnp.mean(state_values * state_values, axis=1, keepdims=True) + epsilon)
        * norm_gain_moe
    ).astype(jnp.bfloat16)
    group_logits = jnp.dot(normed, group_router, preferred_element_type=jnp.float32)
    expert_logits = jnp.dot(normed, expert_router, preferred_element_type=jnp.float32)
    group_total = group_router.shape[1]
    expert_total = expert_router.shape[1]
    per_group = expert_total // group_total
    first_choice = routing[:, 0]
    second_choice = routing[:, 1]
    chosen_group = first_choice // per_group
    group_exp = jnp.exp(group_logits)
    group_match = chosen_group[:, None] == jnp.arange(group_total, dtype=jnp.int32)[None, :]
    group_prob = jnp.sum(jnp.where(group_match, group_exp, jnp.float32(0.0)), axis=1) / jnp.sum(
        group_exp, axis=1
    )
    expert_iota = jnp.arange(expert_total, dtype=jnp.int32)[None, :]
    first_logit = jnp.sum(
        jnp.where(first_choice[:, None] == expert_iota, expert_logits, jnp.float32(0.0)), axis=1
    )
    second_logit = jnp.sum(
        jnp.where(second_choice[:, None] == expert_iota, expert_logits, jnp.float32(0.0)), axis=1
    )
    first_exp = jnp.exp(first_logit)
    second_exp = jnp.exp(second_logit)
    first_weight = group_prob * first_exp / (first_exp + second_exp)
    second_weight = group_prob * second_exp / (first_exp + second_exp)
    row_count = normed.shape[0]
    capacity = 2 * row_count // expert_total
    flat_experts = routing.reshape(-1)
    indicator = (flat_experts[:, None] == expert_iota).astype(jnp.int32)
    before = jnp.cumsum(indicator, axis=0) - indicator
    position = jnp.sum(before * indicator, axis=1)
    destination = flat_experts * capacity + position
    source = (
        jnp.zeros((2 * row_count,), jnp.int32)
        .at[destination]
        .set(jnp.arange(2 * row_count, dtype=jnp.int32) // 2)
    )
    outgoing = normed[source].reshape(expert_total, capacity, normed.shape[1])
    arrived = lax.all_to_all(outgoing, "sp", split_axis=0, concat_axis=0, tiled=True)
    senders, slot_count, features = arrived.shape
    flattened = arrived.reshape(senders * slot_count, features)
    gate_part = jnp.dot(flattened, expert_gate_w[0], preferred_element_type=jnp.float32)
    up_part = jnp.dot(flattened, expert_up_w[0], preferred_element_type=jnp.float32)
    expert_hidden = (jax.nn.silu(gate_part) * up_part).astype(jnp.bfloat16)
    expert_result = jnp.dot(
        expert_hidden, expert_down_w[0], preferred_element_type=jnp.float32
    ).astype(jnp.bfloat16)
    returned = lax.all_to_all(
        expert_result.reshape(senders, slot_count, features),
        "sp",
        split_axis=0,
        concat_axis=0,
        tiled=True,
    )
    picked = (
        returned.reshape(2 * row_count, normed.shape[1])[destination]
        .reshape(row_count, 2, normed.shape[1])
        .astype(jnp.float32)
    )
    mixture = first_weight[:, None] * picked[:, 0] + second_weight[:, None] * picked[:, 1]
    return (state_values + mixture).astype(jnp.bfloat16)


def solution(mesh):
    placed = (
        P("sp", "tp"),
        P("sp", "tp"),
        P("sp"),
        P(None, "tp"),
        P(),
        P(),
        P("tp", None),
        P(("sp", "tp"), None),
        P(),
        P(),
        P(),
        P(("sp", "tp"), None),
        P("sp", None, None),
        P("sp", None, None),
        P("sp", None, None),
    )
    return jax.shard_map(
        body, mesh=mesh, in_specs=placed, out_specs=P(("sp", "tp"), None), check_vma=False
    )
```

profile of v0, /device:TPU:0, one launch (start us, length us, event | category | flops | bytes accessed | tf_op | source)
XLA Modules:
  0.0 186.5 jit_solution(3365401490658242660)
XLA Ops:
  7.3 0.8 slice.297
  8.0 1.7 collective-permute-start
  9.7 1.8 multiply_convert_fusion.2
  11.5 3.4 %collective-permute-start.1 = (bf16[30,128]{1,0:T(8,128)(2,1)S(1)}, bf16[30,128]{1,0:T(8,128)(2,1)S(1)}, u32[]{:S(2)}, u32[]{:S(2)}) collective-permute-start(bf16[30,128]{1,0:T(8,128)(2,1)S(1)} %slice.402), channel_id=1, source_target_pairs={{0,16},{16,32},{32,48},{48,64},{64,80},{80,96},{96,112},{112,128},... | collective-permute-start | bytes 23048 | tf_op jit(solution)/shard_map/ppermute | solution.py:12
  15.4 0.8 collective-permute-done.1
  16.3 16.6 %add_convert_fusion = bf16[3072,128]{1,0:T(8,128)(2,1)} fusion(bf16[3072,128]{1,0:T(8,128)(2,1)S(1)} %multiply_convert_fusion.2, bf16[30,128]{1,0:T(8,128)(2,1)S(1)} %collective-permute-done.1, f32[128]{0:T(128)S(1)} %get-tuple-element.14, f32[128]{0:T(128)S(1)} %get-tuple-element.15, f32[128]{0:T(128)S(1)} %get-tuple-element.16, ...), kind=kLoop, calls=%fused_computation.60 | loop fusion | flops 83755008 | bytes 1688576 | tf_op jit(solution)/shard_map/convert_element_type | solution.py:60
  32.9 8.7 %all-to-all-start = ((bf16[16,192,128]{2,1,0:T(8,128)(2,1)}), bf16[16,192,128]{2,1,0:T(8,128)(2,1)S(1)}, u32[]{:S(2)}, u32[]{:S(2)}) async-start(bf16[16,192,128]{2,1,0:T(8,128)(2,1)} %bitcast.147), calls=%async_computation | async-start | bytes 1572864 | tf_op jit(solution)/shard_map/all_to_all | solution.py:61
  42.0 0.9 reduce-window.6
  43.5 2.9 %scatter_custom_fusion = s32[384]{0:T(512)S(1)} fusion(s32[384]{0:T(512)S(1)} %fusion.132, s32[384]{0:T(512)S(1)} %add_select_fusion, s32[]{:T(128)} %constant.50.clone.1), kind=kCustom, calls=%fused_computation.261 | custom fusion | bytes 1540 | tf_op jit(solution)/shard_map/scatter | solution.py:112
  46.5 25.0 %all-to-all-done = bf16[16,192,128]{2,1,0:T(8,128)(2,1)S(1)} async-done(((bf16[16,192,128]{2,1,0:T(8,128)(2,1)}), bf16[16,192,128]{2,1,0:T(8,128)(2,1)S(1)}, u32[]{:S(2)}, u32[]{:S(2)}) %all-to-all-start) | async-done | bytes 786464 | tf_op jit(solution)/shard_map/all_to_all | solution.py:61
  72.1 11.1 %all-gather.2.cloned.1.call-done = bf16[2048,2048]{1,0:T(8,128)(2,1)} async-done(((bf16[128,2048]{1,0:T(8,128)(2,1)}), bf16[2048,2048]{1,0:T(8,128)(2,1)}) %all-gather.2.cloned.1.call-update) | async-done | bytes 8388624 | tf_op jit(solution)/shard_map/all_gather | solution.py:18
  83.2 5.7 %multiply_reduce_fusion = (f32[192]{0:T(256)S(1)}, f32[192,2048]{1,0:T(8,128)S(1)}) fusion(bf16[2048,2048]{1,0:T(8,128)(2,1)} %all-gather.2.cloned.1.call-done, f32[2048]{0:T(1024)S(1)} %copy-done.11, f32[2048]{0:T(1024)S(1)} %copy-done.12, f32[192]{0:T(256)S(1)} %add_rsqrt_fusion.1, f32[192]{0:T(256)S(1)} %broadcast_multiply_fusion.1, ...), kind=kOutput, calls=%fused_computation.58 | convolution fusion | flops 1616903936 | bytes 11553024 | tf_op jit(solution)/shard_map/dot_general | solution.py:16
  88.9 1.1 copy-done.1
  90.2 3.1 %gather_fusion = bf16[384,2048]{1,0:T(8,128)(2,1)} fusion(bf16[192,2048]{1,0:T(8,128)(2,1)S(1)} %multiply_convert_fusion, s32[1024]{0:T(1024)S(1)} %pad_clamp_fusion.1), kind=kCustom, calls=%fused_computation | custom fusion | bytes 3147264 | tf_op jit(solution)/shard_map/gather | solution.py:114
  93.3 30.1 %all_to_all.23 = bf16[16,24,2048]{2,1,0:T(8,128)(2,1)S(1)} all-to-all(bf16[16,24,2048]{2,1,0:T(8,128)(2,1)} %bitcast.146), channel_id=1, replica_groups=mesh['sp'=16,'tp'=16] {'sp'}, dimensions={0} | all-to-all | bytes 3145728 | tf_op jit(solution)/shard_map/all_to_all | solution.py:115
  123.5 1.2 copy-done.3
  124.6 1.9 fusion.5
  126.5 5.3 %convolution_convert_fusion = bf16[384,2048]{1,0:T(8,128)(2,1)} fusion(bf16[1,512,2048]{2,1,0:T(8,128)(2,1)S(1)} %copy-done, bf16[384,2048]{1,0:T(8,128)(2,1)} %bitcast.150, bf16[1,2048,512]{2,1,0:T(8,128)(2,1)} %param.28, f32[384,512]{1,0:T(8,128)} %fusion.5), kind=kOutput, calls=%fused_computation.32 | convolution fusion | flops 1612578816 | bytes 8126464 | tf_op jit(solution)/shard_map/dot_general | solution.py:121
  131.8 4.7 %all-to-all-start.2 = ((bf16[16,24,2048]{2,1,0:T(8,128)(2,1)}), bf16[16,24,2048]{2,1,0:T(8,128)(2,1)}, u32[]{:S(2)}, u32[]{:S(2)}) async-start(bf16[16,24,2048]{2,1,0:T(8,128)(2,1)} %bitcast.148), calls=%async_computation.2 | async-start | bytes 3145728 | tf_op jit(solution)/shard_map/all_to_all | solution.py:124
  137.3 22.2 %all-to-all-done.2 = bf16[16,24,2048]{2,1,0:T(8,128)(2,1)} async-done(((bf16[16,24,2048]{2,1,0:T(8,128)(2,1)}), bf16[16,24,2048]{2,1,0:T(8,128)(2,1)}, u32[]{:S(2)}, u32[]{:S(2)}) %all-to-all-start.2) | async-done | bytes 1572896 | tf_op jit(solution)/shard_map/all_to_all | solution.py:124
  159.5 6.7 %gather_fusion.1 = bf16[384,2048]{1,0:T(8,128)(2,1)} fusion(bf16[384,2048]{1,0:T(8,128)(2,1)} %bitcast.43, s32[1024]{0:T(1024)S(1)} %pad_clamp_fusion), kind=kCustom, calls=%fused_computation.1 | custom fusion | bytes 3147264 | tf_op jit(solution)/shard_map/gather | solution.py:132
  166.2 4.7 %reshape.154 = f32[192,2,2048]{2,1,0:T(2,128)} reshape(bf16[384,2048]{1,0:T(8,128)(2,1)} %gather_fusion.1) | data formatting | bytes 4718592 | tf_op jit(solution)/shard_map/convert_element_type | solution.py:134
  170.9 6.2 %fusion.138 = (f32[192,1,2048]{2,1,0:T(1,128)S(1)}, f32[192,1,2048]{2,1,0:T(1,128)S(1)}) fusion(f32[192,2,2048]{2,1,0:T(2,128)} %reshape.154), kind=kLoop, calls=%fused_computation.302 | loop fusion | bytes 6291456 | tf_op jit(solution)/shard_map/slice | solution.py:136
  177.1 2.6 %fusion.15 = bf16[192,2048]{1,0:T(8,128)(2,1)} fusion(f32[192,2048]{1,0:T(8,128)S(1)} %copy-done.2, f32[192,1,2048]{2,1,0:T(1,128)S(1)} %get-tuple-element.12, f32[192,1,2048]{2,1,0:T(1,128)S(1)} %get-tuple-element.11, f32[192]{0:T(256)S(1)} %multiply_divide_fusion, f32[192]{0:T(256)S(1)} %get-tuple-element.9), kind=kLoop, calls=%fused_computation.54 | loop fusion | flops 1966080 | bytes 5506560 | tf_op jit(solution)/shard_map/convert_element_type | solution.py:137
  (61 shorter events, 3.8 us)
Async XLA Ops:
  6.5 119.9 %copy-start = (bf16[1,512,2048]{2,1,0:T(8,128)(2,1)S(1)}, bf16[1,512,2048]{2,1,0:T(8,128)(2,1)}, u32[]{:S(2)}) copy-start(bf16[1,512,2048]{2,1,0:T(8,128)(2,1)} %param.29) | copy-start | bytes 6291460
  6.5 8.5 %copy-start.4 = (s32[3072]{0:T(1024)S(1)}, s32[3072]{0:T(1024)}, u32[]{:S(2)}) copy-start(s32[3072]{0:T(1024)} %param.17) | copy-start | bytes 36868
  6.5 8.4 %copy-start.9 = (bf16[31,128]{1,0:T(8,128)(2,1)S(1)}, bf16[31,128]{1,0:T(8,128)(2,1)}, u32[]{:S(2)}) copy-start(bf16[31,128]{1,0:T(8,128)(2,1)} %param.18) | copy-start | bytes 23812
  6.5 76.6 %all-gather.2.cloned.1.call-start = ((), (), s32[]{:S(2)}) async-start(), calls=%async_computation.3 | async-start | bytes 8912896 | tf_op jit(solution)/shard_map/all_gather | solution.py:18
  8.0 7.0 %collective-permute-start = (s32[30]{0:T(128)S(1)}, s32[30]{0:T(128)S(1)}, u32[]{:S(2)}, u32[]{:S(2)}) collective-permute-start(s32[30]{0:T(128)S(1)} %slice.297), channel_id=1, source_target_pairs={{0,16},{16,32},{32,48},{48,64},{64,80},{80,96},{96,112},{112,128},... | collective-permute-start | bytes 368 | tf_op jit(solution)/shard_map/ppermute | solution.py:12
  11.5 4.8 %collective-permute-start.1 = (bf16[30,128]{1,0:T(8,128)(2,1)S(1)}, bf16[30,128]{1,0:T(8,128)(2,1)S(1)}, u32[]{:S(2)}, u32[]{:S(2)}) collective-permute-start(bf16[30,128]{1,0:T(8,128)(2,1)S(1)} %slice.402), channel_id=1, source_target_pairs={{0,16},{16,32},{32,48},{48,64},{64,80},{80,96},{96,112},{112,128},... | collective-permute-start | bytes 23048 | tf_op jit(solution)/shard_map/ppermute | solution.py:12
  16.3 25.3 %copy-start.6 = (s32[192,2]{0,1:T(2,128)S(1)}, s32[192,2]{0,1:T(2,128)}, u32[]{:S(2)}) copy-start(s32[192,2]{0,1:T(2,128)} %param.26) | copy-start | bytes 4612
  32.9 50.3 %copy-start.11 = (f32[2048]{0:T(1024)S(1)}, f32[2048]{0:T(1024)}, u32[]{:S(2)}) copy-start(f32[2048]{0:T(1024)} %param.20) | copy-start | bytes 24580
  32.9 50.3 %copy-start.12 = (f32[2048]{0:T(1024)S(1)}, f32[2048]{0:T(1024)}, u32[]{:S(2)}) copy-start(f32[2048]{0:T(1024)} %param.19) | copy-start | bytes 24580
  32.9 38.6 %all-to-all-start = ((bf16[16,192,128]{2,1,0:T(8,128)(2,1)}), bf16[16,192,128]{2,1,0:T(8,128)(2,1)S(1)}, u32[]{:S(2)}, u32[]{:S(2)}) async-start(bf16[16,192,128]{2,1,0:T(8,128)(2,1)} %bitcast.147), calls=%async_computation | async-start | bytes 1572864 | tf_op jit(solution)/shard_map/all_to_all | solution.py:61
  72.1 18.0 %copy-start.7 = (f32[2048]{0:T(1024)S(1)}, f32[2048]{0:T(1024)}, u32[]{:S(2)}) copy-start(f32[2048]{0:T(1024)} %param.23) | copy-start | bytes 24580
  88.9 1.1 copy-start.1
  93.3 31.3 %copy-start.10 = (bf16[1,2048,512]{2,1,0:T(8,128)(2,1)S(1)}, bf16[1,2048,512]{2,1,0:T(8,128)(2,1)}, u32[]{:S(2)}) copy-start(bf16[1,2048,512]{2,1,0:T(8,128)(2,1)} %param.27) | copy-start | bytes 6291460
  123.5 1.2 copy-start.3
  131.8 4.7 %copy-start.8 = (bf16[2048,2]{0,1:T(2,128)(2,1)S(1)}, bf16[2048,2]{0,1:T(2,128)(2,1)}, u32[]{:S(2)}) copy-start(bf16[2048,2]{0,1:T(2,128)(2,1)} %param.24) | copy-start | bytes 24580
  131.8 5.1 %copy-start.5 = (bf16[2048,16]{0,1:T(8,128)(2,1)S(1)}, bf16[2048,16]{0,1:T(8,128)(2,1)}, u32[]{:S(2)}) copy-start(bf16[2048,16]{0,1:T(8,128)(2,1)} %param.25) | copy-start | bytes 196612
  131.8 27.7 %all-to-all-start.2 = ((bf16[16,24,2048]{2,1,0:T(8,128)(2,1)}), bf16[16,24,2048]{2,1,0:T(8,128)(2,1)}, u32[]{:S(2)}, u32[]{:S(2)}) async-start(bf16[16,24,2048]{2,1,0:T(8,128)(2,1)} %bitcast.148), calls=%async_computation.2 | async-start | bytes 3145728 | tf_op jit(solution)/shard_map/all_to_all | solution.py:124
  170.9 6.2 %copy-start.2 = (f32[192,2048]{1,0:T(8,128)S(1)}, f32[192,2048]{1,0:T(8,128)}, u32[]{:S(2)}) copy-start(f32[192,2048]{1,0:T(8,128)} %copy-done.1) | copy-start | bytes 4718596
Sparse Core Ops, SparseCore 0:
  9.2 73.9 all-gather.1
where the time goes:
time: 187 us
  waiting for transfers between devices  59.9 us (32%)
  blocking collectives  30.1 us (16%)
  local copies, waits for them, and re-layouts  27.6 us (15%)
  other arithmetic  23.2 us (12%)
  starting transfers between devices  18.5 us (10%)
  between operations  13.7 us (7%)
  matrix products  13.5 us (7%)
    all_to_all x1, blocking collectives, body(): lax.all_to_all(outgoing, 'sp', split_axis=0, concat_axis=0, tiled=True)  30.1 us
    all_to_all x1, waiting for transfers between devices, body(): lax.all_to_all(convolved, 'tp', split_axis=0, concat_axis=1, tiled=True)  25 us
    all_to_all x1, waiting for transfers between devices, body(): lax.all_to_all(expert_result.reshape(senders, slot_count, features), 'sp'...  22.2 us
    convert_element_type x1, other arithmetic, body(): convolved = summed.astype(jnp.bfloat16)  16.6 us
    all_gather x1, waiting for transfers between devices, project_rows(): lax.all_gather(proj_weight, 'tp', axis=0, tiled=True)  11.1 us
    all_to_all x1, starting transfers between devices, body(): lax.all_to_all(convolved, 'tp', split_axis=0, concat_axis=1, tiled=True)  8.7 us
    gather x1, local copies, waits for them, and re-layouts, body(): returned.reshape(2 * row_count, normed.shape[1])[destination]  6.68 us
    slice x1, local copies, waits for them, and re-layouts, body(): picked[:, 0]  6.18 us
  transfers between devices with their start and end apart: 5, of which 4 were waited for; matrix products, arithmetic and copies ran while one was open for 14% of the time, Pallas kernels for 0%

commit v1 on v0

--- a/solution.py
+++ b/solution.py
@@ -4,6 +4,27 @@
 from jax.sharding import PartitionSpec as P
 
 epsilon = 1e-06
+
+
+def collect(array, axis, dim):
+    length, position, rows = (lax.axis_size(axis), lax.axis_index(axis), array.shape[dim])
+    right = [(i, (i + 1) % length) for i in range(length)]
+    left = [(i, (i - 1) % length) for i in range(length)]
+    filled = jnp.zeros((*array.shape[:dim], length * rows, *array.shape[dim + 1 :]), array.dtype)
+    filled = lax.dynamic_update_slice_in_dim(filled, array, position * rows, axis=dim)
+    from_left = from_right = array
+    half = length // 2
+    for step in range(1, half + 1):
+        from_left = lax.ppermute(from_left, axis, right)
+        filled = lax.dynamic_update_slice_in_dim(
+            filled, from_left, (position - step) % length * rows, axis=dim
+        )
+        if step < length - half:
+            from_right = lax.ppermute(from_right, axis, left)
+            filled = lax.dynamic_update_slice_in_dim(
+                filled, from_right, (position + step) % length * rows, axis=dim
+            )
+    return filled
 
 
 def shifted(array, axis, by):
@@ -14,9 +35,7 @@
 
 def project_rows(activated_rows, proj_weight):
     return jnp.dot(
-        activated_rows,
-        lax.all_gather(proj_weight, "tp", axis=0, tiled=True),
-        preferred_element_type=jnp.float32,
+        activated_rows, collect(proj_weight, "tp", 0), preferred_element_type=jnp.float32
     )
 
 

time: 187 us -> 226 us (1.21); the launches traced: 187 us -> 222 us
  local copies, waits for them, and re-layouts: 27.6 us -> 55 us
  starting transfers between devices: 18.5 us -> 39.3 us
  between operations: 13.7 us -> 0.33 us
  blocking collectives: 30.1 us -> 22.5 us
  other arithmetic: 23.2 us -> 29.7 us
  waiting for transfers between devices: 59.9 us -> 62.2 us
    ppermute x0 -> x15, waiting for transfers between devices: none -> 45.7 us  [the longest x8 41.7 us: collect(): from_left = lax.ppermute(from_left, axis, right)]
    all_to_all x1, waiting for transfers between devices: 25 us -> 0.01 us  [body(): lax.all_to_all(convolved, 'tp', split_axis=0, concat_axis=1, tiled=True)]
    ppermute x0 -> x15, starting transfers between devices: none -> 21.8 us  [the longest x7 21.3 us: collect(): from_right = lax.ppermute(from_right, axis, left)]
    dynamic_update_slice x0 -> x16, local copies, waits for them, and re-layouts: none -> 18.8 us  [the longest x8 11 us: collect(): lax.dynamic_update_slice_in_dim(filled, from_left, (position - step) % le...]
    all_gather x1 -> x0, waiting for transfers between devices: 11.1 us -> none  [project_rows(): lax.all_gather(proj_weight, 'tp', axis=0, tiled=True)]
    all_to_all x1, blocking collectives: 30.1 us -> 22.5 us  [body(): lax.all_to_all(outgoing, 'sp', split_axis=0, concat_axis=0, tiled=True)]
    all_to_all x1, waiting for transfers between devices: 22.2 us -> 16.5 us  [body(): lax.all_to_all(expert_result.reshape(senders, slot_count, features), 'sp'...]
    broadcast_in_dim x0 -> x1, local copies, waits for them, and re-layouts: none -> 4.28 us  [collect(): jnp.zeros((*array.shape[:dim], length * rows, *array.shape[dim + 1:]), ar...]
  transfers between devices with their start and end apart: 5 -> 19, of which waited for: 4 -> 12; matrix products, arithmetic and copies ran while one was open for 14% -> 26% of each run, Pallas kernels for 0% -> 0%
where the time goes in v1:
time: 226 us; the launch traced here: 222 us
  waiting for transfers between devices  62.2 us (28%)
  local copies, waits for them, and re-layouts  55 us (24%)
  starting transfers between devices  39.3 us (17%)
  other arithmetic  29.7 us (13%)
  blocking collectives  22.5 us (10%)
  matrix products  13.4 us (6%)
    ppermute x8, waiting for transfers between devices, collect(): from_left = lax.ppermute(from_left, axis, right)  41.7 us
    all_to_all x1, blocking collectives, body(): lax.all_to_all(outgoing, 'sp', split_axis=0, concat_axis=0, tiled=True)  22.5 us
    ppermute x7, starting transfers between devices, collect(): from_right = lax.ppermute(from_right, axis, left)  21.3 us
    all_to_all x1, waiting for transfers between devices, body(): lax.all_to_all(expert_result.reshape(senders, slot_count, features), 'sp'...  16.5 us
    convert_element_type x1, other arithmetic, body(): convolved = summed.astype(jnp.bfloat16)  16.4 us
    dynamic_update_slice x8, local copies, waits for them, and re-layouts, collect(): lax.dynamic_update_slice_in_dim(filled, from_left, (position - step) % le...  11 us
    dynamic_update_slice x7, local copies, waits for them, and re-layouts, collect(): lax.dynamic_update_slice_in_dim(filled, from_right, (position + step) % l...  6.95 us
    ppermute x2, starting transfers between devices, shifted(): return lax.ppermute(array, axis, pairs)  6.78 us
  transfers between devices with their start and end apart: 19, of which 12 were waited for; matrix products, arithmetic and copies ran while one was open for 26% of the time, Pallas kernels for 0%

profile of v1, /device:TPU:0, one launch (start us, length us, event | category | flops | bytes accessed | tf_op | source)
XLA Modules:
  0.0 222.4 jit_solution(4869977696214443831)
XLA Ops:
  0.0 3.6 %collective-permute-start.3 = (bf16[128,2048]{1,0:T(8,128)(2,1)}, bf16[128,2048]{1,0:T(8,128)(2,1)S(1)}, u32[]{:S(2)}, u32[]{:S(2)}) collective-permute-start(bf16[128,2048]{1,0:T(8,128)(2,1)} %param.21), channel_id=1, source_target_pairs={{0,15},{1,0},{2,1},{3,2},{4,3},{5,4},{6,5},{7,6},{8,7},{9,8},{10,9... | collective-permute-start | bytes 1572872 | tf_op jit(solution)/shard_map/ppermute | solution.py:23
  4.9 3.9 %collective-permute-start = (s32[30]{0:T(128)}, s32[30]{0:T(128)}, u32[]{:S(2)}, u32[]{:S(2)}) collective-permute-start(s32[30]{0:T(128)} %slice.297), channel_id=1, source_target_pairs={{0,16},{16,32},{32,48},{48,64},{64,80},{80,96},{96,112},{112,128},... | collective-permute-start | bytes 368 | tf_op jit(solution)/shard_map/ppermute | solution.py:33
  22.2 3.1 %scatter_custom_fusion = s32[384]{0:T(512)S(1)} fusion(s32[384]{0:T(512)S(1)} %fusion.132, s32[384]{0:T(512)} %add_select_fusion, s32[]{:T(128)} %constant.138.clone.1), kind=kCustom, calls=%fused_computation.277 | custom fusion | bytes 2048 | tf_op jit(solution)/shard_map/scatter | solution.py:131
  29.4 16.4 %add_convert_fusion = bf16[3072,128]{1,0:T(8,128)(2,1)} fusion(bf16[3072,128]{1,0:T(8,128)(2,1)S(1)} %multiply_convert_fusion.2, bf16[30,128]{1,0:T(8,128)(2,1)S(1)} %collective-permute-done.1, f32[128]{0:T(128)} %get-tuple-element.14, f32[128]{0:T(128)} %get-tuple-element.15, f32[128]{0:T(128)} %get-tuple-element.16, f32[128]{0:T(128)} %get-tuple-element.17, ...), kind=kLoop, calls=%fused_computation.60 | loop fusion | flops 83755008 | bytes 1688576 | tf_op jit(solution)/shard_map/convert_element_type | solution.py:79
  45.8 6.2 %all-to-all-start = ((bf16[16,192,128]{2,1,0:T(8,128)(2,1)}), bf16[16,192,128]{2,1,0:T(8,128)(2,1)S(1)}, u32[]{:S(2)}, u32[]{:S(2)}) async-start(bf16[16,192,128]{2,1,0:T(8,128)(2,1)} %bitcast.147), calls=%async_computation | async-start | bytes 1572864 | tf_op jit(solution)/shard_map/all_to_all | solution.py:80
  52.5 4.3 %broadcast_in_dim.280 = bf16[2048,2048]{1,0:T(8,128)(2,1)} broadcast(bf16[]{:T(256)} %constant.135.clone.1), dimensions={} | broadcast | bytes 8388610 | tf_op jit(solution)/shard_map/broadcast_in_dim | solution.py:13
  60.2 18.7 %collective-permute-done.4 = bf16[128,2048]{1,0:T(8,128)(2,1)} collective-permute-done((bf16[128,2048]{1,0:T(8,128)(2,1)}, bf16[128,2048]{1,0:T(8,128)(2,1)}, u32[]{:S(2)}, u32[]{:S(2)}) %collective-permute-start.4) | collective-permute-done | bytes 524320 | tf_op jit(solution)/shard_map/ppermute | solution.py:18
  91.6 3.0 %collective-permute-start.9 = (bf16[128,2048]{1,0:T(8,128)(2,1)S(1)}, bf16[128,2048]{1,0:T(8,128)(2,1)S(1)}, u32[]{:S(2)}, u32[]{:S(2)}) collective-permute-start(bf16[128,2048]{1,0:T(8,128)(2,1)S(1)} %collective-permute-done.7), channel_id=1, source_target_pairs={{0,15},{1,0},{2,1},{3,2},{4,3},{5,4},{6,5},{7,6},{8,7},{9,8},{10,9... | collective-permute-start | bytes 1572872 | tf_op jit(solution)/shard_map/ppermute | solution.py:23
  94.6 4.6 %collective-permute-done.8 = bf16[128,2048]{1,0:T(8,128)(2,1)} collective-permute-done((bf16[128,2048]{1,0:T(8,128)(2,1)}, bf16[128,2048]{1,0:T(8,128)(2,1)}, u32[]{:S(2)}, u32[]{:S(2)}) %collective-permute-start.8) | collective-permute-done | bytes 524320 | tf_op jit(solution)/shard_map/ppermute | solution.py:18
  101.3 3.1 %collective-permute-start.11 = (bf16[128,2048]{1,0:T(8,128)(2,1)S(1)}, bf16[128,2048]{1,0:T(8,128)(2,1)S(1)}, u32[]{:S(2)}, u32[]{:S(2)}) collective-permute-start(bf16[128,2048]{1,0:T(8,128)(2,1)S(1)} %collective-permute-done.9), channel_id=1, source_target_pairs={{0,15},{1,0},{2,1},{3,2},{4,3},{5,4},{6,5},{7,6},{8,7},{9,8},{10,9... | collective-permute-start | bytes 1572872 | tf_op jit(solution)/shard_map/ppermute | solution.py:23
  111.9 3.0 %collective-permute-start.13 = (bf16[128,2048]{1,0:T(8,128)(2,1)S(1)}, bf16[128,2048]{1,0:T(8,128)(2,1)S(1)}, u32[]{:S(2)}, u32[]{:S(2)}) collective-permute-start(bf16[128,2048]{1,0:T(8,128)(2,1)S(1)} %collective-permute-done.11), channel_id=1, source_target_pairs={{0,15},{1,0},{2,1},{3,2},{4,3},{5,4},{6,5},{7,6},{8,7},{9,8},{10,9... | collective-permute-start | bytes 1572872 | tf_op jit(solution)/shard_map/ppermute | solution.py:23
  115.7 3.3 %collective-permute-done.12 = bf16[128,2048]{1,0:T(8,128)(2,1)S(1)} collective-permute-done((bf16[128,2048]{1,0:T(8,128)(2,1)S(1)}, bf16[128,2048]{1,0:T(8,128)(2,1)S(1)}, u32[]{:S(2)}, u32[]{:S(2)}) %collective-permute-start.12) | collective-permute-done | bytes 524320 | tf_op jit(solution)/shard_map/ppermute | solution.py:18
  121.6 3.1 %collective-permute-start.15 = (bf16[128,2048]{1,0:T(8,128)(2,1)S(1)}, bf16[128,2048]{1,0:T(8,128)(2,1)S(1)}, u32[]{:S(2)}, u32[]{:S(2)}) collective-permute-start(bf16[128,2048]{1,0:T(8,128)(2,1)S(1)} %collective-permute-done.13), channel_id=1, source_target_pairs={{0,15},{1,0},{2,1},{3,2},{4,3},{5,4},{6,5},{7,6},{8,7},{9,8},{10,9... | collective-permute-start | bytes 1572872 | tf_op jit(solution)/shard_map/ppermute | solution.py:23
  125.6 3.2 %collective-permute-done.14 = bf16[128,2048]{1,0:T(8,128)(2,1)S(1)} collective-permute-done((bf16[128,2048]{1,0:T(8,128)(2,1)S(1)}, bf16[128,2048]{1,0:T(8,128)(2,1)S(1)}, u32[]{:S(2)}, u32[]{:S(2)}) %collective-permute-start.14) | collective-permute-done | bytes 524320 | tf_op jit(solution)/shard_map/ppermute | solution.py:18
  132.2 6.4 %collective-permute-done.16 = bf16[128,2048]{1,0:T(8,128)(2,1)S(1)} collective-permute-done((bf16[128,2048]{1,0:T(8,128)(2,1)S(1)}, bf16[128,2048]{1,0:T(8,128)(2,1)S(1)}, u32[]{:S(2)}, u32[]{:S(2)}) %collective-permute-start.16) | collective-permute-done | bytes 524320 | tf_op jit(solution)/shard_map/ppermute | solution.py:18
  139.5 5.6 %multiply_reduce_fusion = (f32[192]{0:T(256)S(1)}, f32[192,2048]{1,0:T(8,128)S(1)}) fusion(bf16[2048,2048]{1,0:T(8,128)(2,1)} %constant_dynamic-update-slice_fusion, f32[2048]{0:T(1024)S(1)} %copy-done.15, f32[2048]{0:T(1024)S(1)} %copy-done.16, f32[192]{0:T(256)S(1)} %add_rsqrt_fusion.1, f32[192]{0:T(256)S(1)} %broadcast_multiply_fusion.1, ...), kind=kOutput, calls=%fused_computation.58 | convolution fusion | flops 1616903936 | bytes 11553024 | tf_op jit(solution)/shard_map/dot_general | solution.py:37
  146.4 3.1 %gather_fusion = bf16[384,2048]{1,0:T(8,128)(2,1)} fusion(bf16[192,2048]{1,0:T(8,128)(2,1)S(1)} %multiply_convert_fusion, s32[1024]{0:T(1024)S(1)} %pad_clamp_fusion.1), kind=kCustom, calls=%fused_computation | custom fusion | bytes 3147264 | tf_op jit(solution)/shard_map/gather | solution.py:133
  149.6 22.5 %all_to_all.23 = bf16[16,24,2048]{2,1,0:T(8,128)(2,1)S(1)} all-to-all(bf16[16,24,2048]{2,1,0:T(8,128)(2,1)} %bitcast.146), channel_id=1, replica_groups=mesh['sp'=16,'tp'=16] {'sp'}, dimensions={0} | all-to-all | bytes 3145728 | tf_op jit(solution)/shard_map/all_to_all | solution.py:134
  175.1 5.3 %convolution_convert_fusion = bf16[384,2048]{1,0:T(8,128)(2,1)} fusion(bf16[1,512,2048]{2,1,0:T(8,128)(2,1)S(1)} %copy-done, bf16[384,2048]{1,0:T(8,128)(2,1)} %bitcast.150, bf16[1,2048,512]{2,1,0:T(8,128)(2,1)} %param.28, f32[384,512]{1,0:T(8,128)} %fusion.5), kind=kOutput, calls=%fused_computation.32 | convolution fusion | flops 1612578816 | bytes 8126464 | tf_op jit(solution)/shard_map/dot_general | solution.py:140
  180.4 4.5 %all-to-all-start.2 = ((bf16[16,24,2048]{2,1,0:T(8,128)(2,1)}), bf16[16,24,2048]{2,1,0:T(8,128)(2,1)}, u32[]{:S(2)}, u32[]{:S(2)}) async-start(bf16[16,24,2048]{2,1,0:T(8,128)(2,1)} %bitcast.148), calls=%async_computation.2 | async-start | bytes 3145728 | tf_op jit(solution)/shard_map/all_to_all | solution.py:143
  185.7 16.5 %all-to-all-done.2 = bf16[16,24,2048]{2,1,0:T(8,128)(2,1)} async-done(((bf16[16,24,2048]{2,1,0:T(8,128)(2,1)}), bf16[16,24,2048]{2,1,0:T(8,128)(2,1)}, u32[]{:S(2)}, u32[]{:S(2)}) %all-to-all-start.2) | async-done | bytes 1572896 | tf_op jit(solution)/shard_map/all_to_all | solution.py:143
  202.2 6.7 %gather_fusion.1 = bf16[384,2048]{1,0:T(8,128)(2,1)} fusion(bf16[384,2048]{1,0:T(8,128)(2,1)} %bitcast.43, s32[1024]{0:T(1024)S(1)} %pad_clamp_fusion), kind=kCustom, calls=%fused_computation.1 | custom fusion | bytes 3147264 | tf_op jit(solution)/shard_map/gather | solution.py:151
  208.9 4.7 %reshape.154 = f32[192,2,2048]{2,1,0:T(2,128)} reshape(bf16[384,2048]{1,0:T(8,128)(2,1)} %gather_fusion.1) | data formatting | bytes 4718592 | tf_op jit(solution)/shard_map/convert_element_type | solution.py:153
  213.6 6.2 %fusion.138 = (f32[192,1,2048]{2,1,0:T(1,128)S(1)}, f32[192,1,2048]{2,1,0:T(1,128)S(1)}) fusion(f32[192,2,2048]{2,1,0:T(2,128)} %reshape.154), kind=kLoop, calls=%fused_computation.318 | loop fusion | bytes 6291456 | tf_op jit(solution)/shard_map/slice | solution.py:155
  (113 shorter events, 61.0 us)
Async XLA Ops:
  0.0 175.1 %copy-start = (bf16[1,512,2048]{2,1,0:T(8,128)(2,1)S(1)}, bf16[1,512,2048]{2,1,0:T(8,128)(2,1)}, u32[]{:S(2)}) copy-start(bf16[1,512,2048]{2,1,0:T(8,128)(2,1)} %param.29) | copy-start | bytes 6291460
  0.0 25.3 %copy-start.5 = (s32[3072]{0:T(1024)S(1)}, s32[3072]{0:T(1024)}, u32[]{:S(2)}) copy-start(s32[3072]{0:T(1024)} %param.17) | copy-start | bytes 36868
  0.0 14.1 %copy-start.10 = (bf16[31,128]{1,0:T(8,128)(2,1)S(1)}, bf16[31,128]{1,0:T(8,128)(2,1)}, u32[]{:S(2)}) copy-start(bf16[31,128]{1,0:T(8,128)(2,1)} %param.18) | copy-start | bytes 23812
  0.0 15.4 %copy-start.7 = (s32[192,2]{0,1:T(2,128)S(1)}, s32[192,2]{0,1:T(2,128)}, u32[]{:S(2)}) copy-start(s32[192,2]{0,1:T(2,128)} %param.26) | copy-start | bytes 4612
  0.0 52.0 %collective-permute-start.2 = (bf16[128,2048]{1,0:T(8,128)(2,1)}, bf16[128,2048]{1,0:T(8,128)(2,1)}, u32[]{:S(2)}, u32[]{:S(2)}) collective-permute-start(bf16[128,2048]{1,0:T(8,128)(2,1)} %param.21), channel_id=1, source_target_pairs={{0,1},{1,2},{2,3},{3,4},{4,5},{5,6},{6,7},{7,8},{8,9},{9,10},{10,1... | collective-permute-start | bytes 1572872 | tf_op jit(solution)/shard_map/ppermute | solution.py:18
  0.0 57.5 %collective-permute-start.3 = (bf16[128,2048]{1,0:T(8,128)(2,1)}, bf16[128,2048]{1,0:T(8,128)(2,1)S(1)}, u32[]{:S(2)}, u32[]{:S(2)}) collective-permute-start(bf16[128,2048]{1,0:T(8,128)(2,1)} %param.21), channel_id=1, source_target_pairs={{0,15},{1,0},{2,1},{3,2},{4,3},{5,4},{6,5},{7,6},{8,7},{9,8},{10,9... | collective-permute-start | bytes 1572872 | tf_op jit(solution)/shard_map/ppermute | solution.py:23
  4.9 20.3 %collective-permute-start = (s32[30]{0:T(128)}, s32[30]{0:T(128)}, u32[]{:S(2)}, u32[]{:S(2)}) collective-permute-start(s32[30]{0:T(128)} %slice.297), channel_id=1, source_target_pairs={{0,16},{16,32},{32,48},{48,64},{64,80},{80,96},{96,112},{112,128},... | collective-permute-start | bytes 368 | tf_op jit(solution)/shard_map/ppermute | solution.py:33
  11.3 18.2 %collective-permute-start.1 = (bf16[30,128]{1,0:T(8,128)(2,1)}, bf16[30,128]{1,0:T(8,128)(2,1)S(1)}, u32[]{:S(2)}, u32[]{:S(2)}) collective-permute-start(bf16[30,128]{1,0:T(8,128)(2,1)} %slice.402), channel_id=1, source_target_pairs={{0,16},{16,32},{32,48},{48,64},{64,80},{80,96},{96,112},{112,128},... | collective-permute-start | bytes 23048 | tf_op jit(solution)/shard_map/ppermute | solution.py:33
  45.8 45.1 %all-to-all-start = ((bf16[16,192,128]{2,1,0:T(8,128)(2,1)}), bf16[16,192,128]{2,1,0:T(8,128)(2,1)S(1)}, u32[]{:S(2)}, u32[]{:S(2)}) async-start(bf16[16,192,128]{2,1,0:T(8,128)(2,1)} %bitcast.147), calls=%async_computation | async-start | bytes 1572864 | tf_op jit(solution)/shard_map/all_to_all | solution.py:80
  52.0 26.9 %collective-permute-start.4 = (bf16[128,2048]{1,0:T(8,128)(2,1)}, bf16[128,2048]{1,0:T(8,128)(2,1)}, u32[]{:S(2)}, u32[]{:S(2)}) collective-permute-start(bf16[128,2048]{1,0:T(8,128)(2,1)} %collective-permute-done.2), channel_id=1, source_target_pairs={{0,1},{1,2},{2,3},{3,4},{4,5},{5,6},{6,7},{7,8},{8,9},{9,10},{10,1... | collective-permute-start | bytes 1572872 | tf_op jit(solution)/shard_map/ppermute | solution.py:18
  57.6 24.1 %collective-permute-start.5 = (bf16[128,2048]{1,0:T(8,128)(2,1)S(1)}, bf16[128,2048]{1,0:T(8,128)(2,1)}, u32[]{:S(2)}, u32[]{:S(2)}) collective-permute-start(bf16[128,2048]{1,0:T(8,128)(2,1)S(1)} %collective-permute-done.3), channel_id=1, source_target_pairs={{0,15},{1,0},{2,1},{3,2},{4,3},{5,4},{6,5},{7,6},{8,7},{9,8},{10,9... | collective-permute-start | bytes 1572872 | tf_op jit(solution)/shard_map/ppermute | solution.py:23
  78.9 10.1 %collective-permute-start.6 = (bf16[128,2048]{1,0:T(8,128)(2,1)}, bf16[128,2048]{1,0:T(8,128)(2,1)}, u32[]{:S(2)}, u32[]{:S(2)}) collective-permute-start(bf16[128,2048]{1,0:T(8,128)(2,1)} %collective-permute-done.4), channel_id=1, source_target_pairs={{0,1},{1,2},{2,3},{3,4},{4,5},{5,6},{6,7},{7,8},{8,9},{9,10},{10,1... | collective-permute-start | bytes 1572872 | tf_op jit(solution)/shard_map/ppermute | solution.py:18
  81.7 9.9 %collective-permute-start.7 = (bf16[128,2048]{1,0:T(8,128)(2,1)}, bf16[128,2048]{1,0:T(8,128)(2,1)S(1)}, u32[]{:S(2)}, u32[]{:S(2)}) collective-permute-start(bf16[128,2048]{1,0:T(8,128)(2,1)} %collective-permute-done.5), channel_id=1, source_target_pairs={{0,15},{1,0},{2,1},{3,2},{4,3},{5,4},{6,5},{7,6},{8,7},{9,8},{10,9... | collective-permute-start | bytes 1572872 | tf_op jit(solution)/shard_map/ppermute | solution.py:23
  89.0 10.1 %collective-permute-start.8 = (bf16[128,2048]{1,0:T(8,128)(2,1)}, bf16[128,2048]{1,0:T(8,128)(2,1)}, u32[]{:S(2)}, u32[]{:S(2)}) collective-permute-start(bf16[128,2048]{1,0:T(8,128)(2,1)} %collective-permute-done.6), channel_id=1, source_target_pairs={{0,1},{1,2},{2,3},{3,4},{4,5},{5,6},{6,7},{7,8},{8,9},{9,10},{10,1... | collective-permute-start | bytes 1572872 | tf_op jit(solution)/shard_map/ppermute | solution.py:18
  91.6 9.7 %collective-permute-start.9 = (bf16[128,2048]{1,0:T(8,128)(2,1)S(1)}, bf16[128,2048]{1,0:T(8,128)(2,1)S(1)}, u32[]{:S(2)}, u32[]{:S(2)}) collective-permute-start(bf16[128,2048]{1,0:T(8,128)(2,1)S(1)} %collective-permute-done.7), channel_id=1, source_target_pairs={{0,15},{1,0},{2,1},{3,2},{4,3},{5,4},{6,5},{7,6},{8,7},{9,8},{10,9... | collective-permute-start | bytes 1572872 | tf_op jit(solution)/shard_map/ppermute | solution.py:23
  99.2 10.0 %collective-permute-start.10 = (bf16[128,2048]{1,0:T(8,128)(2,1)}, bf16[128,2048]{1,0:T(8,128)(2,1)S(1)}, u32[]{:S(2)}, u32[]{:S(2)}) collective-permute-start(bf16[128,2048]{1,0:T(8,128)(2,1)} %collective-permute-done.8), channel_id=1, source_target_pairs={{0,1},{1,2},{2,3},{3,4},{4,5},{5,6},{6,7},{7,8},{8,9},{9,10},{10,1... | collective-permute-start | bytes 1572872 | tf_op jit(solution)/shard_map/ppermute | solution.py:18
  101.3 10.6 %collective-permute-start.11 = (bf16[128,2048]{1,0:T(8,128)(2,1)S(1)}, bf16[128,2048]{1,0:T(8,128)(2,1)S(1)}, u32[]{:S(2)}, u32[]{:S(2)}) collective-permute-start(bf16[128,2048]{1,0:T(8,128)(2,1)S(1)} %collective-permute-done.9), channel_id=1, source_target_pairs={{0,15},{1,0},{2,1},{3,2},{4,3},{5,4},{6,5},{7,6},{8,7},{9,8},{10,9... | collective-permute-start | bytes 1572872 | tf_op jit(solution)/shard_map/ppermute | solution.py:23
  109.2 9.8 %collective-permute-start.12 = (bf16[128,2048]{1,0:T(8,128)(2,1)S(1)}, bf16[128,2048]{1,0:T(8,128)(2,1)S(1)}, u32[]{:S(2)}, u32[]{:S(2)}) collective-permute-start(bf16[128,2048]{1,0:T(8,128)(2,1)S(1)} %collective-permute-done.10), channel_id=1, source_target_pairs={{0,1},{1,2},{2,3},{3,4},{4,5},{5,6},{6,7},{7,8},{8,9},{9,10},{10,1... | collective-permute-start | bytes 1572872 | tf_op jit(solution)/shard_map/ppermute | solution.py:18
  111.9 9.7 %collective-permute-start.13 = (bf16[128,2048]{1,0:T(8,128)(2,1)S(1)}, bf16[128,2048]{1,0:T(8,128)(2,1)S(1)}, u32[]{:S(2)}, u32[]{:S(2)}) collective-permute-start(bf16[128,2048]{1,0:T(8,128)(2,1)S(1)} %collective-permute-done.11), channel_id=1, source_target_pairs={{0,15},{1,0},{2,1},{3,2},{4,3},{5,4},{6,5},{7,6},{8,7},{9,8},{10,9... | collective-permute-start | bytes 1572872 | tf_op jit(solution)/shard_map/ppermute | solution.py:23
  119.0 9.8 %collective-permute-start.14 = (bf16[128,2048]{1,0:T(8,128)(2,1)S(1)}, bf16[128,2048]{1,0:T(8,128)(2,1)S(1)}, u32[]{:S(2)}, u32[]{:S(2)}) collective-permute-start(bf16[128,2048]{1,0:T(8,128)(2,1)S(1)} %collective-permute-done.12), channel_id=1, source_target_pairs={{0,1},{1,2},{2,3},{3,4},{4,5},{5,6},{6,7},{7,8},{8,9},{9,10},{10,1... | collective-permute-start | bytes 1572872 | tf_op jit(solution)/shard_map/ppermute | solution.py:18
  121.6 9.8 %collective-permute-start.15 = (bf16[128,2048]{1,0:T(8,128)(2,1)S(1)}, bf16[128,2048]{1,0:T(8,128)(2,1)S(1)}, u32[]{:S(2)}, u32[]{:S(2)}) collective-permute-start(bf16[128,2048]{1,0:T(8,128)(2,1)S(1)} %collective-permute-done.13), channel_id=1, source_target_pairs={{0,15},{1,0},{2,1},{3,2},{4,3},{5,4},{6,5},{7,6},{8,7},{9,8},{10,9... | collective-permute-start | bytes 1572872 | tf_op jit(solution)/shard_map/ppermute | solution.py:23
  128.8 9.8 %collective-permute-start.16 = (bf16[128,2048]{1,0:T(8,128)(2,1)S(1)}, bf16[128,2048]{1,0:T(8,128)(2,1)S(1)}, u32[]{:S(2)}, u32[]{:S(2)}) collective-permute-start(bf16[128,2048]{1,0:T(8,128)(2,1)S(1)} %collective-permute-done.14), channel_id=1, source_target_pairs={{0,1},{1,2},{2,3},{3,4},{4,5},{5,6},{6,7},{7,8},{8,9},{9,10},{10,1... | collective-permute-start | bytes 1572872 | tf_op jit(solution)/shard_map/ppermute | solution.py:18
  149.6 23.6 %copy-start.13 = (bf16[1,2048,512]{2,1,0:T(8,128)(2,1)S(1)}, bf16[1,2048,512]{2,1,0:T(8,128)(2,1)}, u32[]{:S(2)}) copy-start(bf16[1,2048,512]{2,1,0:T(8,128)(2,1)} %param.27) | copy-start | bytes 6291460
  180.4 21.9 %all-to-all-start.2 = ((bf16[16,24,2048]{2,1,0:T(8,128)(2,1)}), bf16[16,24,2048]{2,1,0:T(8,128)(2,1)}, u32[]{:S(2)}, u32[]{:S(2)}) async-start(bf16[16,24,2048]{2,1,0:T(8,128)(2,1)} %bitcast.148), calls=%async_computation.2 | async-start | bytes 3145728 | tf_op jit(solution)/shard_map/all_to_all | solution.py:143
  (12 other events, 66.1 us)
